TPU v7x, 32 devices: a whole 2x2x4 slice. The times are simulated.
32 devices in a mesh: rep: 2 (over y), fs: 4 (over z), tp: 4 (over x, core).
Axes of the slice: x: 2, y: 2, z: 4, core: 2. Of those that a mesh axis runs over, the one named last changes fastest.
Arguments:
- stream: bfloat16 [4096, 2048], P(('rep', 'fs', 'tp')), may hold values from -6 to 6
- gain_before: float32 [2048], replicated, may hold values from 0.1 to 1.9
- gain_after: float32 [2048], replicated, may hold values from 0.1 to 1.9
- proj_gate: bfloat16 [2048, 3584], P('fs', 'tp'), may hold values from -0.125 to 0.125
- proj_lift: bfloat16 [2048, 3584], P('fs', 'tp'), may hold values from -0.125 to 0.125
- proj_down: bfloat16 [3584, 2048], P('tp', 'fs'), may hold values from -0.09375 to 0.09375
- mixer_gain: float32 [2048], replicated, may hold values from 0.1 to 1.9
- mixer_u: bfloat16 [2048, 2048], P('fs', 'tp'), may hold values from -0.125 to 0.125
- mixer_v: bfloat16 [2048, 2048], P('fs', 'tp'), may hold values from -1 to 1
- layer_gain: float32 [2048], P('tp'), may hold values from 0.1 to 1.9
- layer_shift: float32 [2048], P('tp'), may hold values from -3 to 3
- spatial: bfloat16 [16, 128, 128], P('tp'), may hold values from -0.5 to 0.5
- spatial_shift: float32 [16, 128], P('tp'), may hold values from 0.2 to 2
- mixer_down: bfloat16 [2048, 2048], P('tp', 'fs'), may hold values from -0.125 to 0.125
Outputs:
- result: bfloat16 [4096, 2048], P(('rep', 'fs', 'tp'))
All inputs are finite; a program needn't handle non-finite values.
Results may differ from a plain program's by a relative error of at most 0.017.
Values may be sent and summed in bfloat16 or wider, within the bound.
A program may use at most 128 MiB of HBM per device.

v0:
```python
import jax
import jax.numpy as jnp
from jax import lax
from jax.sharding import PartitionSpec as P

GROUP_DIM = 128
SPAN = 128
A = 2048
norm_epsilon = 1e-06
layer_epsilon = 1e-05


def norm_rows(row_block, scale_gain):
    widened = row_block.astype(jnp.float32)
    factor = lax.rsqrt(jnp.mean(widened * widened, axis=1, keepdims=True) + norm_epsilon)
    return (widened * factor * scale_gain).astype(jnp.bfloat16)


def gathered_norm(stream_rows, scale_gain):
    gathered = lax.all_gather(stream_rows, "tp", axis=0, tiled=True)
    return norm_rows(gathered, scale_gain)


def pair_adder(normed, pieces):
    return (
        jnp.dot(normed, pieces[0], preferred_element_type=jnp.float32),
        jnp.dot(normed, pieces[1], preferred_element_type=jnp.float32),
    )


def activate(gate_vals, lift_vals):
    return (jax.nn.silu(gate_vals) * lift_vals).astype(jnp.bfloat16)


def half_again(stream_rows, scale_gain, proj_gate, proj_lift, proj_down):
    normed = gathered_norm(stream_rows, scale_gain)
    gate_vals, lift_vals = pair_adder(
        normed,
        (
            lax.all_gather(proj_gate, "fs", axis=0, tiled=True),
            lax.all_gather(proj_lift, "fs", axis=0, tiled=True),
        ),
    )
    hidden = activate(gate_vals, lift_vals)
    partial_value = jnp.dot(
        hidden,
        lax.all_gather(proj_down, "fs", axis=1, tiled=True),
        preferred_element_type=jnp.float32,
    )
    summed = lax.psum_scatter(
        partial_value.astype(jnp.bfloat16), "tp", scatter_dimension=0, tiled=True
    ).astype(jnp.float32)
    return (stream_rows.astype(jnp.float32) + 0.5 * summed).astype(jnp.bfloat16)


def token_mixer(
    stream_rows,
    mixer_gain,
    mixer_u,
    mixer_v,
    layer_gain,
    layer_shift,
    spatial,
    spatial_shift,
    mixer_down,
):
    gathered = lax.all_gather(stream_rows, "tp", axis=0, tiled=True)
    normed = norm_rows(gathered, mixer_gain)
    seq_tokens = normed.shape[0]
    u_vals, v_vals = pair_adder(
        normed,
        (
            lax.all_gather(mixer_u, "fs", axis=0, tiled=True),
            lax.all_gather(mixer_v, "fs", axis=0, tiled=True),
        ),
    )
    lifted = jax.nn.gelu(v_vals)
    moments = lax.psum((jnp.sum(lifted, axis=1), jnp.sum(lifted * lifted, axis=1)), "tp")
    centre = moments[0] / A
    spread = moments[1] / A - centre * centre
    normed_v = (
        (lifted - centre[:, None]) * lax.rsqrt(spread[:, None] + layer_epsilon) * layer_gain
        + layer_shift
    ).astype(jnp.bfloat16)
    groups_here = spatial.shape[0]
    blocked = normed_v.reshape(seq_tokens // SPAN, SPAN, groups_here, GROUP_DIM)
    causal = jnp.tril(jnp.ones((SPAN, SPAN), dtype=bool))
    masked = jnp.where(causal[None], spatial, jnp.zeros((), jnp.bfloat16))
    mixed_v = jnp.einsum("gts,bsgd->btgd", masked, blocked, preferred_element_type=jnp.float32)
    mixed_v = mixed_v + spatial_shift.T[None, :, :, None]
    gated = (jax.nn.gelu(u_vals) * mixed_v.reshape(seq_tokens, groups_here * GROUP_DIM)).astype(
        jnp.bfloat16
    )
    partial_value = jnp.dot(
        gated,
        lax.all_gather(mixer_down, "fs", axis=1, tiled=True),
        preferred_element_type=jnp.float32,
    )
    summed = lax.psum_scatter(
        partial_value.astype(jnp.bfloat16), "tp", scatter_dimension=0, tiled=True
    ).astype(jnp.float32)
    return (stream_rows.astype(jnp.float32) + summed).astype(jnp.bfloat16)


def body(
    stream,
    gain_before,
    gain_after,
    proj_gate,
    proj_lift,
    proj_down,
    mixer_gain,
    mixer_u,
    mixer_v,
    layer_gain,
    layer_shift,
    spatial,
    spatial_shift,
    mixer_down,
):
    first = half_again(stream, gain_before, proj_gate, proj_lift, proj_down)
    second = token_mixer(
        first,
        mixer_gain,
        mixer_u,
        mixer_v,
        layer_gain,
        layer_shift,
        spatial,
        spatial_shift,
        mixer_down,
    )
    result = half_again(second, gain_after, proj_gate, proj_lift, proj_down)
    return result


def solution(mesh):
    placed = (
        P(("rep", "fs", "tp"), None),
        P(),
        P(),
        P("fs", "tp"),
        P("fs", "tp"),
        P("tp", "fs"),
        P(),
        P("fs", "tp"),
        P("fs", "tp"),
        P("tp"),
        P("tp"),
        P("tp", None, None),
        P("tp", None),
        P("tp", "fs"),
    )
    return jax.shard_map(
        body, mesh=mesh, in_specs=placed, out_specs=P(("rep", "fs", "tp"), None), check_vma=False
    )
```

profile of v0, /device:TPU:0, one launch (start us, length us, event | category | flops | bytes accessed | tf_op | source)
XLA Modules:
  0.0 575.2 jit_solution(15976335767558670113)
XLA Ops:
  9.4 24.8 %all-gather.10.cloned.1.call-done = bf16[512,2048]{1,0:T(8,128)(2,1)} async-done(((bf16[128,2048]{1,0:T(8,128)(2,1)}), bf16[512,2048]{1,0:T(8,128)(2,1)}) %all-gather.10.cloned.1.call-update) | async-done | bytes 2097168 | tf_op jit(solution)/shard_map/all_gather | solution.py:20
  34.2 2.2 fusion
  36.4 71.5 %all-gather.12.cloned.1.call-done = bf16[2048,896]{1,0:T(8,128)(2,1)} async-done(((bf16[512,896]{1,0:T(8,128)(2,1)}), bf16[2048,896]{1,0:T(8,128)(2,1)}) %all-gather.12.cloned.1.call-update) | async-done | bytes 3670032 | tf_op jit(solution)/shard_map/all_gather | solution.py:40
  107.9 5.6 fusion.42
  113.5 66.6 %all-gather.14.cloned.1.call-done = bf16[2048,896]{1,0:T(8,128)(2,1)} async-done(((bf16[512,896]{1,0:T(8,128)(2,1)}), bf16[2048,896]{1,0:T(8,128)(2,1)}) %all-gather.14.cloned.1.call-update) | async-done | bytes 3670032 | tf_op jit(solution)/shard_map/all_gather | solution.py:41
  180.2 72.1 %all-gather.16.cloned.1.call-done = bf16[896,2048]{1,0:T(8,128)(2,1)} async-done(((bf16[896,512]{1,0:T(8,128)(2,1)}), bf16[896,2048]{1,0:T(8,128)(2,1)}) %all-gather.16.cloned.1.call-update) | async-done | bytes 3670032 | tf_op jit(solution)/shard_map/all_gather | solution.py:47
  252.3 9.7 %convolution_convert_fusion.1 = bf16[512,2048]{1,0:T(8,128)(2,1)} fusion(bf16[896,2048]{1,0:T(8,128)(2,1)} %all-gather.16.cloned.1.call-done, f32[512,896]{1,0:T(8,128)} %fusion.42, bf16[2048,896]{1,0:T(8,128)(2,1)} %all-gather.14.cloned.1.call-done, bf16[512,2048]{1,0:T(8,128)(2,1)S(1)} %copy-done.4, f32[2048]{0:T(1024)S(1)} %copy-done.10, ...), kind=kOutput, calls=%fused_computation.16 | convolution fusion | flops 3766091776 | bytes 13379584 | tf_op jit(solution)/shard_map/dot_general | solution.py:45
  262.0 29.9 %reduce-scatter.4.cloned.1.call-done = bf16[128,2048]{1,0:T(8,128)(2,1)} async-done(((bf16[512,2048]{1,0:T(8,128)(2,1)}), bf16[128,2048]{1,0:T(8,128)(2,1)}) %reduce-scatter.4.cloned.1.call-update) | async-done | bytes 524304 | tf_op jit(solution)/shard_map/reduce_scatter | solution.py:50
  291.9 2.0 add_convert_fusion.3
  296.2 20.4 %all-gather.18.cloned.1.call-done = bf16[512,2048]{1,0:T(8,128)(2,1)} async-done(((bf16[128,2048]{1,0:T(8,128)(2,1)}), bf16[512,2048]{1,0:T(8,128)(2,1)}) %all-gather.18.cloned.1.call-update) | async-done | bytes 2097168 | tf_op jit(solution)/shard_map/all_gather | solution.py:67
  316.6 2.2 fusion.3
  318.9 45.0 %all-gather.22.cloned.1.call-done = bf16[2048,512]{1,0:T(8,128)(2,1)} async-done(((bf16[512,512]{1,0:T(8,128)(2,1)}), bf16[2048,512]{1,0:T(8,128)(2,1)}) %all-gather.22.cloned.1.call-update) | async-done | bytes 2097168 | tf_op jit(solution)/shard_map/all_gather | solution.py:74
  363.9 4.1 fusion.60
  368.0 6.5 %all-reduce = (f32[512]{0:T(512)S(1)}, f32[512]{0:T(512)S(1)}) all-reduce(f32[512]{0:T(512)S(1)} %get-tuple-element.6, f32[512]{0:T(512)S(1)} %get-tuple-element.5), channel_id=1, replica_groups=mesh['rep'=2,'fs'=4,'tp'=4] {'tp'}, use_global_device_ids=true, to_apply=%region_6.7 | all-reduce | flops 1024 | bytes 8192 | tf_op jit(solution)/shard_map/psum | solution.py:78
  379.7 30.2 %all-gather.20.cloned.1.call-done = bf16[2048,512]{1,0:T(8,128)(2,1)} async-done(((bf16[512,512]{1,0:T(8,128)(2,1)}), bf16[2048,512]{1,0:T(8,128)(2,1)}) %all-gather.20.cloned.1.call-update) | async-done | bytes 2097168 | tf_op jit(solution)/shard_map/all_gather | solution.py:73
  409.9 46.1 %all-gather.24.cloned.1.call-done = bf16[512,2048]{1,0:T(8,128)(2,1)} async-done(((bf16[512,512]{1,0:T(8,128)(2,1)}), bf16[512,2048]{1,0:T(8,128)(2,1)}) %all-gather.24.cloned.1.call-update) | async-done | bytes 2097168 | tf_op jit(solution)/shard_map/all_gather | solution.py:96
  456.0 6.5 %convolution_convert_fusion.2 = bf16[512,2048]{1,0:T(8,128)(2,1)} fusion(bf16[512,2048]{1,0:T(8,128)(2,1)} %all-gather.24.cloned.1.call-done, f32[64,8,4,128]{3,2,1,0:T(4,128)} %bitcast.25, bf16[2048,512]{1,0:T(8,128)(2,1)} %all-gather.20.cloned.1.call-done, bf16[512,2048]{1,0:T(8,128)(2,1)S(1)} %copy-done.3, f32[2048]{0:T(1024)S(1)} %copy-done.11, ...), kind=kOutput, calls=%fused_computation.17 | convolution fusion | flops 2155347968 | bytes 9447424 | tf_op jit(solution)/shard_map/dot_general | solution.py:94
  462.6 30.1 %reduce-scatter.6.cloned.1.call-done = bf16[128,2048]{1,0:T(8,128)(2,1)} async-done(((bf16[512,2048]{1,0:T(8,128)(2,1)}), bf16[128,2048]{1,0:T(8,128)(2,1)}) %reduce-scatter.6.cloned.1.call-update) | async-done | bytes 524304 | tf_op jit(solution)/shard_map/reduce_scatter | solution.py:99
  494.9 22.5 %all-gather.26.cloned.1.call-done = bf16[512,2048]{1,0:T(8,128)(2,1)} async-done(((bf16[128,2048]{1,0:T(8,128)(2,1)}), bf16[512,2048]{1,0:T(8,128)(2,1)}) %all-gather.26.cloned.1.call-update) | async-done | bytes 2097168 | tf_op jit(solution)/shard_map/all_gather | solution.py:20
  517.4 2.2 fusion.6
  519.6 5.7 fusion.28
  525.3 9.7 %convolution_convert_fusion = bf16[512,2048]{1,0:T(8,128)(2,1)} fusion(bf16[896,2048]{1,0:T(8,128)(2,1)} %all-gather.16.cloned.1.call-done, f32[512,896]{1,0:T(8,128)} %fusion.28, bf16[2048,896]{1,0:T(8,128)(2,1)} %all-gather.14.cloned.1.call-done, bf16[512,2048]{1,0:T(8,128)(2,1)S(1)} %copy-done.5, f32[2048]{0:T(1024)S(1)} %copy-done.12, ...), kind=kOutput, calls=%fused_computation.15 | convolution fusion | flops 3766091776 | bytes 13379584 | tf_op jit(solution)/shard_map/dot_general | solution.py:45
  535.0 31.3 %reduce-scatter.8.cloned.1.call-done = bf16[128,2048]{1,0:T(8,128)(2,1)} async-done(((bf16[512,2048]{1,0:T(8,128)(2,1)}), bf16[128,2048]{1,0:T(8,128)(2,1)}) %reduce-scatter.8.cloned.1.call-update) | async-done | bytes 524304 | tf_op jit(solution)/shard_map/reduce_scatter | solution.py:50
  566.4 2.0 add_convert_fusion
  (60 shorter events, 12.6 us)
Async XLA Ops:
  6.5 27.7 %all-gather.10.cloned.1.call-start = ((), (), s32[]{:S(2)}) async-start(), calls=%async_computation.3 | async-start | bytes 2621440 | tf_op jit(solution)/shard_map/all_gather | solution.py:20
  7.3 100.6 %all-gather.12.cloned.1.call-start = ((), (), s32[]{:S(2)}) async-start(), calls=%async_computation.4 | async-start | bytes 4587520 | tf_op jit(solution)/shard_map/all_gather | solution.py:40
  8.0 99.9 %copy-start.10 = (f32[2048]{0:T(1024)S(1)}, f32[2048]{0:T(1024)}, u32[]{:S(2)}) copy-start(f32[2048]{0:T(1024)} %param.15) | copy-start | bytes 24580
  8.0 172.2 %all-gather.14.cloned.1.call-start = ((), (), s32[]{:S(2)}) async-start(), calls=%async_computation.5 | async-start | bytes 4587520 | tf_op jit(solution)/shard_map/all_gather | solution.py:41
  8.8 243.5 %all-gather.16.cloned.1.call-start = ((), (), s32[]{:S(2)}) async-start(), calls=%async_computation.6 | async-start | bytes 4587520 | tf_op jit(solution)/shard_map/all_gather | solution.py:47
  9.3 282.6 %reduce-scatter.4.cloned.1.call-start = ((), (), s32[]{:S(2)}) async-start(), calls=%async_computation.7 | async-start | bytes 2621440 | tf_op jit(solution)/shard_map/reduce_scatter | solution.py:50
  34.2 73.7 %copy-start.4 = (bf16[512,2048]{1,0:T(8,128)(2,1)S(1)}, bf16[512,2048]{1,0:T(8,128)(2,1)}, u32[]{:S(2)}) copy-start(bf16[512,2048]{1,0:T(8,128)(2,1)} %all-gather.10.cloned.1.call-done) | copy-start | bytes 6291460
  262.0 29.9 %copy-start.2 = (bf16[128,2048]{1,0:T(8,128)(2,1)S(1)}, bf16[128,2048]{1,0:T(8,128)(2,1)}, u32[]{:S(2)}) copy-start(bf16[128,2048]{1,0:T(8,128)(2,1)} %param.14) | copy-start | bytes 1572868
  262.0 54.6 %all-gather.18.cloned.1.call-start = ((), (), s32[]{:S(2)}) async-start(), calls=%async_computation.8 | async-start | bytes 2621440 | tf_op jit(solution)/shard_map/all_gather | solution.py:67
  293.9 70.0 %copy-start.11 = (f32[2048]{0:T(1024)S(1)}, f32[2048]{0:T(1024)}, u32[]{:S(2)}) copy-start(f32[2048]{0:T(1024)} %param.20) | copy-start | bytes 24580
  293.9 70.0 %all-gather.22.cloned.1.call-start = ((), (), s32[]{:S(2)}) async-start(), calls=%async_computation.10 | async-start | bytes 2621440 | tf_op jit(solution)/shard_map/all_gather | solution.py:74
  294.7 115.3 %all-gather.20.cloned.1.call-start = ((), (), s32[]{:S(2)}) async-start(), calls=%async_computation.9 | async-start | bytes 2621440 | tf_op jit(solution)/shard_map/all_gather | solution.py:73
  295.4 160.6 %all-gather.24.cloned.1.call-start = ((), (), s32[]{:S(2)}) async-start(), calls=%async_computation.11 | async-start | bytes 2621440 | tf_op jit(solution)/shard_map/all_gather | solution.py:96
  296.2 196.5 %reduce-scatter.6.cloned.1.call-start = ((), (), s32[]{:S(2)}) async-start(), calls=%async_computation.12 | async-start | bytes 2621440 | tf_op jit(solution)/shard_map/reduce_scatter | solution.py:99
  316.6 47.3 %copy-start.3 = (bf16[512,2048]{1,0:T(8,128)(2,1)S(1)}, bf16[512,2048]{1,0:T(8,128)(2,1)}, u32[]{:S(2)}) copy-start(bf16[512,2048]{1,0:T(8,128)(2,1)} %all-gather.18.cloned.1.call-done) | copy-start | bytes 6291460
  318.9 55.7 %copy-start.7 = (f32[512]{0:T(512)S(1)}, f32[512]{0:T(512)}, u32[]{:S(2)}) copy-start(f32[512]{0:T(512)} %param.24) | copy-start | bytes 6148
  318.9 55.7 %copy-start.8 = (f32[512]{0:T(512)S(1)}, f32[512]{0:T(512)}, u32[]{:S(2)}) copy-start(f32[512]{0:T(512)} %param.23) | copy-start | bytes 6148
  368.0 8.9 %copy-start.6 = (bf16[4,128,128]{2,1,0:T(8,128)(2,1)S(1)}, bf16[4,128,128]{2,1,0:T(8,128)(2,1)}, u32[]{:S(2)}) copy-start(bf16[4,128,128]{2,1,0:T(8,128)(2,1)} %param.25) | copy-start | bytes 393220
  368.0 8.9 %copy-start.9 = (f32[4,128]{1,0:T(4,128)S(1)}, f32[4,128]{1,0:T(4,128)}, u32[]{:S(2)}) copy-start(f32[4,128]{1,0:T(4,128)} %param.26) | copy-start | bytes 6148
  462.5 30.2 %copy-start = (bf16[128,2048]{1,0:T(8,128)(2,1)S(1)}, bf16[128,2048]{1,0:T(8,128)(2,1)}, u32[]{:S(2)}) copy-start(bf16[128,2048]{1,0:T(8,128)(2,1)} %add_convert_fusion.3) | copy-start | bytes 1572868
  462.5 57.1 %copy-start.12 = (f32[2048]{0:T(1024)S(1)}, f32[2048]{0:T(1024)}, u32[]{:S(2)}) copy-start(f32[2048]{0:T(1024)} %param.16) | copy-start | bytes 24580
  462.5 54.8 %all-gather.26.cloned.1.call-start = ((), (), s32[]{:S(2)}) async-start(), calls=%async_computation.13 | async-start | bytes 2621440 | tf_op jit(solution)/shard_map/all_gather | solution.py:20
  494.6 71.7 %reduce-scatter.8.cloned.1.call-start = ((), (), s32[]{:S(2)}) async-start(), calls=%async_computation.14 | async-start | bytes 2621440 | tf_op jit(solution)/shard_map/reduce_scatter | solution.py:50
  535.0 31.4 %copy-start.1 = (bf16[128,2048]{1,0:T(8,128)(2,1)S(1)}, bf16[128,2048]{1,0:T(8,128)(2,1)}, u32[]{:S(2)}) copy-start(bf16[128,2048]{1,0:T(8,128)(2,1)} %add_convert_fusion.1) | copy-start | bytes 1572868
  (1 other events, 2.2 us)
Sparse Core Ops, SparseCore 0:
  8.9 25.2 all-gather.9
  35.8 72.0 all-gather.11
  109.5 70.6 all-gather.13
  181.6 70.6 all-gather.15
  262.1 29.7 reduce-scatter.3
  294.1 22.5 all-gather.17
  318.2 45.6 all-gather.21
  365.5 44.4 all-gather.19
  411.5 44.4 all-gather.23
  462.6 29.9 reduce-scatter.5
  494.8 22.5 all-gather.25
  535.1 31.1 reduce-scatter.7
where the time goes:
time: 576 us; the launch traced here: 575 us
  waiting for transfers between devices  495 us (86%)
  matrix products  42.7 us (7%)
  other arithmetic  14.1 us (2%)
  between operations  13.7 us (2%)
  blocking collectives  6.51 us (1%)
    all_gather x1, waiting for transfers between devices, half_again(): lax.all_gather(proj_down, 'fs', axis=1, tiled=True)  72.1 us
    all_gather x1, waiting for transfers between devices, half_again(): lax.all_gather(proj_gate, 'fs', axis=0, tiled=True)  71.5 us
    all_gather x1, waiting for transfers between devices, half_again(): lax.all_gather(proj_lift, 'fs', axis=0, tiled=True)  66.6 us
    reduce_scatter x2, waiting for transfers between devices, half_again(): lax.psum_scatter(partial_value.astype(jnp.bfloat16), 'tp', scatter_dimens...  61.2 us
    all_gather x2, waiting for transfers between devices, gathered_norm(): gathered = lax.all_gather(stream_rows, 'tp', axis=0, tiled=True)  47.3 us
    all_gather x1, waiting for transfers between devices, token_mixer(): lax.all_gather(mixer_down, 'fs', axis=1, tiled=True)  46.1 us
    all_gather x1, waiting for transfers between devices, token_mixer(): lax.all_gather(mixer_v, 'fs', axis=0, tiled=True)  45 us
    all_gather x1, waiting for transfers between devices, token_mixer(): lax.all_gather(mixer_u, 'fs', axis=0, tiled=True)  30.2 us
  transfers between devices with their start and end apart: 12, of which 12 were waited for; matrix products, arithmetic and copies ran while one was open for 3% of the time, Pallas kernels for 0%

commit v1 on v0

--- a/solution.py
+++ b/solution.py
@@ -17,7 +17,15 @@
 
 
 def gathered_norm(stream_rows, scale_gain):
-    gathered = lax.all_gather(stream_rows, "tp", axis=0, tiled=True)
+    ways, here = (lax.axis_size("tp"), lax.axis_index("tp"))
+    grown, reach = (stream_rows, 1)
+    while reach < ways:
+        theirs = lax.ppermute(grown, "tp", [(d, d ^ reach) for d in range(ways)])
+        mine_first = jnp.concatenate([grown, theirs], axis=0)
+        theirs_first = jnp.concatenate([theirs, grown], axis=0)
+        grown = jnp.where(here & reach == 0, mine_first, theirs_first)
+        reach = 2 * reach
+    gathered = grown
     return norm_rows(gathered, scale_gain)
 
 

time: 576 us -> 552 us (0.958)
  waiting for transfers between devices: 495 us -> 473 us
    ppermute x0 -> x4, waiting for transfers between devices: none -> 51.7 us  [gathered_norm(): theirs = lax.ppermute(grown, 'tp', [(d, d ^ reach) for d in range(ways)])]
    all_gather x2 -> x0, waiting for transfers between devices: 47.3 us -> none  [gathered_norm(): gathered = lax.all_gather(stream_rows, 'tp', axis=0, tiled=True)]
    all_gather x1, waiting for transfers between devices: 71.5 us -> 45.5 us  [half_again(): lax.all_gather(proj_gate, 'fs', axis=0, tiled=True)]
  transfers between devices with their start and end apart: 12 -> 14, of which waited for: 12 -> 14; matrix products, arithmetic and copies ran while one was open for 3% -> 3% of each run, Pallas kernels for 0% -> 0%
where the time goes in v1:
time: 552 us
  waiting for transfers between devices  473 us (86%)
  matrix products  40.7 us (7%)
  between operations  13.7 us (2%)
  other arithmetic  10.9 us (2%)
  blocking collectives  6.69 us (1%)
    all_gather x1, waiting for transfers between devices, half_again(): lax.all_gather(proj_down, 'fs', axis=1, tiled=True)  72.3 us
    all_gather x1, waiting for transfers between devices, half_again(): lax.all_gather(proj_lift, 'fs', axis=0, tiled=True)  66.6 us
    reduce_scatter x2, waiting for transfers between devices, half_again(): lax.psum_scatter(partial_value.astype(jnp.bfloat16), 'tp', scatter_dimens...  61.2 us
    ppermute x4, waiting for transfers between devices, gathered_norm(): theirs = lax.ppermute(grown, 'tp', [(d, d ^ reach) for d in range(ways)])  51.7 us
    all_gather x1, waiting for transfers between devices, token_mixer(): lax.all_gather(mixer_down, 'fs', axis=1, tiled=True)  46.1 us
    all_gather x1, waiting for transfers between devices, half_again(): lax.all_gather(proj_gate, 'fs', axis=0, tiled=True)  45.5 us
    all_gather x1, waiting for transfers between devices, token_mixer(): lax.all_gather(mixer_v, 'fs', axis=0, tiled=True)  44.9 us
    all_gather x1, waiting for transfers between devices, token_mixer(): lax.all_gather(mixer_u, 'fs', axis=0, tiled=True)  30.1 us
  transfers between devices with their start and end apart: 14, of which 14 were waited for; matrix products, arithmetic and copies ran while one was open for 3% of the time, Pallas kernels for 0%

profile of v1, /device:TPU:0, one launch (start us, length us, event | category | flops | bytes accessed | tf_op | source)
XLA Modules:
  0.0 551.5 jit_solution(7864095533583845701)
XLA Ops:
  11.2 2.9 collective-permute-start.1
  14.1 23.5 %collective-permute-done.1 = bf16[256,2048]{1,0:T(8,128)(2,1)S(1)} collective-permute-done((bf16[256,2048]{1,0:T(8,128)(2,1)S(1)}, bf16[256,2048]{1,0:T(8,128)(2,1)S(1)}, u32[]{:S(2)}, u32[]{:S(2)}) %collective-permute-start.1) | collective-permute-done | bytes 1048608 | tf_op jit(solution)/shard_map/ppermute | solution.py:23
  38.3 45.5 %all-gather.8.cloned.1.call-done = bf16[2048,896]{1,0:T(8,128)(2,1)} async-done(((bf16[512,896]{1,0:T(8,128)(2,1)}), bf16[2048,896]{1,0:T(8,128)(2,1)}) %all-gather.8.cloned.1.call-update) | async-done | bytes 3670032 | tf_op jit(solution)/shard_map/all_gather | solution.py:48
  83.8 5.7 %fusion.42 = f32[512,896]{1,0:T(8,128)} fusion(bf16[2048,896]{1,0:T(8,128)(2,1)} %all-gather.8.cloned.1.call-done, f32[2048]{0:T(1024)S(1)} %copy-done.8, f32[512]{0:T(512)S(1)} %add_rsqrt_fusion.3, bf16[256,2048]{1,0:T(8,128)(2,1)S(1)} %collective-permute-done.1, bf16[256,2048]{1,0:T(8,128)(2,1)S(1)} %maximum_select_fusion.2, pred[]{:T(512)S(6)} %eq.8), kind=kOutput, calls=%fused_computation.52 | convolution fusion | flops 1892679680 | bytes 7612417 | tf_op jit(solution)/shard_map/dot_general | solution.py:34
  89.4 66.6 %all-gather.10.cloned.1.call-done = bf16[2048,896]{1,0:T(8,128)(2,1)} async-done(((bf16[512,896]{1,0:T(8,128)(2,1)}), bf16[2048,896]{1,0:T(8,128)(2,1)}) %all-gather.10.cloned.1.call-update) | async-done | bytes 3670032 | tf_op jit(solution)/shard_map/all_gather | solution.py:49
  156.0 72.3 %all-gather.12.cloned.1.call-done = bf16[896,2048]{1,0:T(8,128)(2,1)} async-done(((bf16[896,512]{1,0:T(8,128)(2,1)}), bf16[896,2048]{1,0:T(8,128)(2,1)}) %all-gather.12.cloned.1.call-update) | async-done | bytes 3670032 | tf_op jit(solution)/shard_map/all_gather | solution.py:55
  228.3 9.7 %convolution_convert_fusion.1 = bf16[512,2048]{1,0:T(8,128)(2,1)} fusion(bf16[896,2048]{1,0:T(8,128)(2,1)} %all-gather.12.cloned.1.call-done, f32[512,896]{1,0:T(8,128)} %fusion.42, bf16[2048,896]{1,0:T(8,128)(2,1)} %all-gather.10.cloned.1.call-done, f32[2048]{0:T(1024)S(1)} %copy-done.8, f32[512]{0:T(512)S(1)} %add_rsqrt_fusion.3, ...), kind=kOutput, calls=%fused_computation.16 | convolution fusion | flops 3775528960 | bytes 13379585 | tf_op jit(solution)/shard_map/dot_general | solution.py:53
  238.0 29.9 %reduce-scatter.4.cloned.1.call-done = bf16[128,2048]{1,0:T(8,128)(2,1)} async-done(((bf16[512,2048]{1,0:T(8,128)(2,1)}), bf16[128,2048]{1,0:T(8,128)(2,1)}) %reduce-scatter.4.cloned.1.call-update) | async-done | bytes 524304 | tf_op jit(solution)/shard_map/reduce_scatter | solution.py:58
  267.9 2.0 add_convert_fusion.3
  272.1 20.6 %all-gather.14.cloned.1.call-done = bf16[512,2048]{1,0:T(8,128)(2,1)} async-done(((bf16[128,2048]{1,0:T(8,128)(2,1)}), bf16[512,2048]{1,0:T(8,128)(2,1)}) %all-gather.14.cloned.1.call-update) | async-done | bytes 2097168 | tf_op jit(solution)/shard_map/all_gather | solution.py:75
  292.6 2.2 fusion.3
  294.9 44.9 %all-gather.18.cloned.1.call-done = bf16[2048,512]{1,0:T(8,128)(2,1)} async-done(((bf16[512,512]{1,0:T(8,128)(2,1)}), bf16[2048,512]{1,0:T(8,128)(2,1)}) %all-gather.18.cloned.1.call-update) | async-done | bytes 2097168 | tf_op jit(solution)/shard_map/all_gather | solution.py:82
  339.8 4.1 fusion.60
  343.9 6.7 %all-reduce = (f32[512]{0:T(512)S(1)}, f32[512]{0:T(512)S(1)}) all-reduce(f32[512]{0:T(512)S(1)} %get-tuple-element.6, f32[512]{0:T(512)S(1)} %get-tuple-element.5), channel_id=1, replica_groups=mesh['rep'=2,'fs'=4,'tp'=4] {'tp'}, use_global_device_ids=true, to_apply=%region_6.7 | all-reduce | flops 1024 | bytes 8192 | tf_op jit(solution)/shard_map/psum | solution.py:86
  355.7 30.1 %all-gather.16.cloned.1.call-done = bf16[2048,512]{1,0:T(8,128)(2,1)} async-done(((bf16[512,512]{1,0:T(8,128)(2,1)}), bf16[2048,512]{1,0:T(8,128)(2,1)}) %all-gather.16.cloned.1.call-update) | async-done | bytes 2097168 | tf_op jit(solution)/shard_map/all_gather | solution.py:81
  385.8 46.1 %all-gather.20.cloned.1.call-done = bf16[512,2048]{1,0:T(8,128)(2,1)} async-done(((bf16[512,512]{1,0:T(8,128)(2,1)}), bf16[512,2048]{1,0:T(8,128)(2,1)}) %all-gather.20.cloned.1.call-update) | async-done | bytes 2097168 | tf_op jit(solution)/shard_map/all_gather | solution.py:104
  431.9 6.5 %convolution_convert_fusion.2 = bf16[512,2048]{1,0:T(8,128)(2,1)} fusion(bf16[512,2048]{1,0:T(8,128)(2,1)} %all-gather.20.cloned.1.call-done, f32[64,8,4,128]{3,2,1,0:T(4,128)} %bitcast.25, bf16[2048,512]{1,0:T(8,128)(2,1)} %all-gather.16.cloned.1.call-done, bf16[512,2048]{1,0:T(8,128)(2,1)S(1)} %copy-done.2, f32[2048]{0:T(1024)S(1)} %copy-done.9, ...), kind=kOutput, calls=%fused_computation.17 | convolution fusion | flops 2155347968 | bytes 9447424 | tf_op jit(solution)/shard_map/dot_general | solution.py:102
  438.4 30.1 %reduce-scatter.6.cloned.1.call-done = bf16[128,2048]{1,0:T(8,128)(2,1)} async-done(((bf16[512,2048]{1,0:T(8,128)(2,1)}), bf16[128,2048]{1,0:T(8,128)(2,1)}) %reduce-scatter.6.cloned.1.call-update) | async-done | bytes 524304 | tf_op jit(solution)/shard_map/reduce_scatter | solution.py:107
  469.8 1.9 collective-permute-done.2
  472.4 24.9 %collective-permute-done.3 = bf16[256,2048]{1,0:T(8,128)(2,1)S(1)} collective-permute-done((bf16[256,2048]{1,0:T(8,128)(2,1)S(1)}, bf16[256,2048]{1,0:T(8,128)(2,1)S(1)}, u32[]{:S(2)}, u32[]{:S(2)}) %collective-permute-start.3) | collective-permute-done | bytes 1048608 | tf_op jit(solution)/shard_map/ppermute | solution.py:23
  498.0 3.6 fusion.28
  501.6 9.7 %convolution_convert_fusion = bf16[512,2048]{1,0:T(8,128)(2,1)} fusion(bf16[896,2048]{1,0:T(8,128)(2,1)} %all-gather.12.cloned.1.call-done, f32[512,896]{1,0:T(8,128)} %fusion.28, bf16[2048,896]{1,0:T(8,128)(2,1)} %all-gather.10.cloned.1.call-done, f32[2048]{0:T(1024)S(1)} %copy-done.10, f32[512]{0:T(512)S(1)} %add_rsqrt_fusion, ...), kind=kOutput, calls=%fused_computation.15 | convolution fusion | flops 3775528960 | bytes 13379585 | tf_op jit(solution)/shard_map/dot_general | solution.py:53
  511.3 31.3 %reduce-scatter.8.cloned.1.call-done = bf16[128,2048]{1,0:T(8,128)(2,1)} async-done(((bf16[512,2048]{1,0:T(8,128)(2,1)}), bf16[128,2048]{1,0:T(8,128)(2,1)}) %reduce-scatter.8.cloned.1.call-update) | async-done | bytes 524304 | tf_op jit(solution)/shard_map/reduce_scatter | solution.py:58
  542.7 2.0 add_convert_fusion
  (60 shorter events, 15.4 us)
Async XLA Ops:
  6.5 77.2 %all-gather.8.cloned.1.call-start = ((), (), s32[]{:S(2)}) async-start(), calls=%async_computation.3 | async-start | bytes 4587520 | tf_op jit(solution)/shard_map/all_gather | solution.py:48
  7.3 148.8 %all-gather.10.cloned.1.call-start = ((), (), s32[]{:S(2)}) async-start(), calls=%async_computation.4 | async-start | bytes 4587520 | tf_op jit(solution)/shard_map/all_gather | solution.py:49
  8.0 220.3 %all-gather.12.cloned.1.call-start = ((), (), s32[]{:S(2)}) async-start(), calls=%async_computation.5 | async-start | bytes 4587520 | tf_op jit(solution)/shard_map/all_gather | solution.py:55
  8.7 259.2 %reduce-scatter.4.cloned.1.call-start = ((), (), s32[]{:S(2)}) async-start(), calls=%async_computation.6 | async-start | bytes 2621440 | tf_op jit(solution)/shard_map/reduce_scatter | solution.py:58
  8.8 2.1 collective-permute-start
  9.4 74.4 %copy-start.8 = (f32[2048]{0:T(1024)S(1)}, f32[2048]{0:T(1024)}, u32[]{:S(2)}) copy-start(f32[2048]{0:T(1024)} %param.15) | copy-start | bytes 24580
  11.2 26.4 %collective-permute-start.1 = (bf16[256,2048]{1,0:T(8,128)(2,1)S(1)}, bf16[256,2048]{1,0:T(8,128)(2,1)S(1)}, u32[]{:S(2)}, u32[]{:S(2)}) collective-permute-start(bf16[256,2048]{1,0:T(8,128)(2,1)S(1)} %maximum_select_fusion.2), channel_id=1, source_target_pairs={{0,2},{1,3},{2,0},{3,1},{4,6},{5,7},{6,4},{7,5},{8,10},{9,11},{10,... | collective-permute-start | bytes 3145736 | tf_op jit(solution)/shard_map/ppermute | solution.py:23
  238.0 54.6 %all-gather.14.cloned.1.call-start = ((), (), s32[]{:S(2)}) async-start(), calls=%async_computation.7 | async-start | bytes 2621440 | tf_op jit(solution)/shard_map/all_gather | solution.py:75
  269.9 69.9 %copy-start.9 = (f32[2048]{0:T(1024)S(1)}, f32[2048]{0:T(1024)}, u32[]{:S(2)}) copy-start(f32[2048]{0:T(1024)} %param.20) | copy-start | bytes 24580
  269.9 69.8 %all-gather.18.cloned.1.call-start = ((), (), s32[]{:S(2)}) async-start(), calls=%async_computation.9 | async-start | bytes 2621440 | tf_op jit(solution)/shard_map/all_gather | solution.py:82
  270.5 115.3 %all-gather.16.cloned.1.call-start = ((), (), s32[]{:S(2)}) async-start(), calls=%async_computation.8 | async-start | bytes 2621440 | tf_op jit(solution)/shard_map/all_gather | solution.py:81
  271.3 160.6 %all-gather.20.cloned.1.call-start = ((), (), s32[]{:S(2)}) async-start(), calls=%async_computation.10 | async-start | bytes 2621440 | tf_op jit(solution)/shard_map/all_gather | solution.py:104
  272.0 196.5 %reduce-scatter.6.cloned.1.call-start = ((), (), s32[]{:S(2)}) async-start(), calls=%async_computation.11 | async-start | bytes 2621440 | tf_op jit(solution)/shard_map/reduce_scatter | solution.py:107
  292.6 47.1 %copy-start.2 = (bf16[512,2048]{1,0:T(8,128)(2,1)S(1)}, bf16[512,2048]{1,0:T(8,128)(2,1)}, u32[]{:S(2)}) copy-start(bf16[512,2048]{1,0:T(8,128)(2,1)} %all-gather.14.cloned.1.call-done) | copy-start | bytes 6291460
  294.9 55.7 %copy-start.4 = (f32[512]{0:T(512)S(1)}, f32[512]{0:T(512)}, u32[]{:S(2)}) copy-start(f32[512]{0:T(512)} %param.24) | copy-start | bytes 6148
  294.9 55.7 %copy-start.5 = (f32[512]{0:T(512)S(1)}, f32[512]{0:T(512)}, u32[]{:S(2)}) copy-start(f32[512]{0:T(512)} %param.23) | copy-start | bytes 6148
  343.9 9.1 %copy-start.3 = (bf16[4,128,128]{2,1,0:T(8,128)(2,1)S(1)}, bf16[4,128,128]{2,1,0:T(8,128)(2,1)}, u32[]{:S(2)}) copy-start(bf16[4,128,128]{2,1,0:T(8,128)(2,1)} %param.25) | copy-start | bytes 393220
  343.9 9.1 %copy-start.6 = (f32[4,128]{1,0:T(4,128)S(1)}, f32[4,128]{1,0:T(4,128)}, u32[]{:S(2)}) copy-start(f32[4,128]{1,0:T(4,128)} %param.26) | copy-start | bytes 6148
  438.4 30.2 %copy-start = (bf16[128,2048]{1,0:T(8,128)(2,1)S(1)}, bf16[128,2048]{1,0:T(8,128)(2,1)}, u32[]{:S(2)}) copy-start(bf16[128,2048]{1,0:T(8,128)(2,1)} %add_convert_fusion.3) | copy-start | bytes 1572868
  438.4 104.3 %reduce-scatter.8.cloned.1.call-start = ((), (), s32[]{:S(2)}) async-start(), calls=%async_computation.12 | async-start | bytes 2621440 | tf_op jit(solution)/shard_map/reduce_scatter | solution.py:58
  469.7 28.3 %copy-start.7 = (bf16[2048,896]{1,0:T(8,128)(2,1)S(1)}, bf16[2048,896]{1,0:T(8,128)(2,1)}, u32[]{:S(2)}) copy-start(bf16[2048,896]{1,0:T(8,128)(2,1)} %all-gather.8.cloned.1.call-done) | copy-start | bytes 11010052
  469.7 28.3 %copy-start.10 = (f32[2048]{0:T(1024)S(1)}, f32[2048]{0:T(1024)}, u32[]{:S(2)}) copy-start(f32[2048]{0:T(1024)} %param.16) | copy-start | bytes 24580
  469.7 2.0 collective-permute-start.2
  471.9 25.3 %collective-permute-start.3 = (bf16[256,2048]{1,0:T(8,128)(2,1)S(1)}, bf16[256,2048]{1,0:T(8,128)(2,1)S(1)}, u32[]{:S(2)}, u32[]{:S(2)}) collective-permute-start(bf16[256,2048]{1,0:T(8,128)(2,1)S(1)} %maximum_select_fusion.3), channel_id=1, source_target_pairs={{0,2},{1,3},{2,0},{3,1},{4,6},{5,7},{6,4},{7,5},{8,10},{9,11},{10,... | collective-permute-start | bytes 3145736 | tf_op jit(solution)/shard_map/ppermute | solution.py:23
  (1 other events, 2.3 us)
Sparse Core Ops, SparseCore 0:
  8.9 74.8 all-gather.7
  85.3 70.6 all-gather.9
  157.6 70.6 all-gather.11
  238.1 29.7 reduce-scatter.3
  270.0 22.5 all-gather.13
  294.1 45.6 all-gather.17
  341.3 44.4 all-gather.15
  387.4 44.4 all-gather.19
  438.5 29.9 reduce-scatter.5
  511.5 31.1 reduce-scatter.7
